TPU v7x, 32 devices: a whole 2x2x4 slice. The times are simulated.
32 devices in a mesh: ep: 8 (over z, x), tp: 4 (over y, core).
Axes of the slice: x: 2, y: 2, z: 4, core: 2. Of those that a mesh axis runs over, the one named last changes fastest.
Arguments:
- tokens: bfloat16 [64, 2048], P('ep'), may hold values from -6 to 6
- mix_gain: bfloat16 [2048], replicated, may hold values from 0.099609375 to 1.8984375
- w_query: bfloat16 [2048, 512], P(None, 'tp'), may hold values from -0.125 to 0.125
- w_key: bfloat16 [2048, 512], P(None, 'tp'), may hold values from -0.125 to 0.125
- w_value: bfloat16 [2048, 512], P(None, 'tp'), may hold values from -0.125 to 0.125
- w_igate: bfloat16 [2048, 4], replicated, may hold values from -0.125 to 0.125
- w_fgate: bfloat16 [2048, 4], replicated, may hold values from -0.125 to 0.125
- forget_bias: float32 [4], replicated, may hold values from 0.5 to 4.5
- w_out: bfloat16 [512, 2048], P('tp'), may hold values from -0.25 to 0.25
- mem_state: float32 [64, 4, 16384], P('ep', 'tp'), may hold values from -0.75 to 0.75
- norm_state: float32 [64, 512], P('ep', 'tp'), may hold values from -0.75 to 0.75
- max_state: float32 [64, 4], P('ep', 'tp'), may hold values from -3 to 3
- ffn_gain: bfloat16 [2048], replicated, may hold values from 0.099609375 to 1.8984375
- route_ids: int32 [64, 2], P('ep'), may hold values from 0 to 7, all different within a row; in each aligned block of 8 rows (0 to 7, 8 to 15, ...) at most 3 rows name the same one
- route_weights: float32 [64, 2], P('ep'), may hold values from 0.1 to 1
- w_gate: bfloat16 [2048, 32768], P(None, ('ep', 'tp')), may hold values from -0.125 to 0.125
- w_up: bfloat16 [2048, 32768], P(None, ('ep', 'tp')), may hold values from -0.125 to 0.125
- w_down: bfloat16 [32768, 2048], P('ep', 'tp'), may hold values from -0.09375 to 0.09375
Outputs:
- out_tokens: bfloat16 [64, 2048], P('ep', 'tp')
- new_memory: float32 [64, 4, 16384], P('ep', 'tp')
- new_norm: float32 [64, 512], P('ep', 'tp')
- new_max: float32 [64, 4], P('ep', 'tp')
Inputs may be any that keep to these rules, and one draw needn't show every extreme that they name: `route_ids`: each row names 2 different experts; among the rows of one index of ep no expert is named more than 3 times, a bound that some block reaches.
All inputs are finite; a program needn't handle non-finite values.
Results may differ from a plain program's by a relative error of at most 0.013.
The roundings to bfloat16 on the way count: a program that leaves them out, or rounds other values in their place, can miss the bound.
Values may be sent and summed in bfloat16 or wider, within the bound.
A program may use at most 64 MiB of HBM per device.

v0:
```python
import jax
import jax.numpy as jnp
from jax import lax
from jax.sharding import PartitionSpec as P

FF = 4096
epsilon = 1e-06


def scaled_rows(row_data, squares, feature_count, gain_values):
    factor = lax.rsqrt(squares / feature_count + epsilon)
    return (row_data * factor[:, None] * gain_values.astype(jnp.float32)).astype(jnp.bfloat16)


def rounded_wide(matrix):
    return lax.optimization_barrier(matrix.astype(jnp.bfloat16)).astype(jnp.float32)


def shards(
    tokens,
    mix_gain,
    w_query,
    w_key,
    w_value,
    w_igate,
    w_fgate,
    forget_bias,
    w_out,
    mem_state,
    norm_state,
    max_state,
    ffn_gain,
    route_ids,
    route_weights,
    w_gate,
    w_up,
    w_down,
):
    seq_count, model_width = tokens.shape
    local_heads = mem_state.shape[1]
    head_dim = norm_state.shape[1] // local_heads
    tp_count = lax.axis_size("tp")
    tp_at = lax.axis_index("tp")
    ep_count = lax.axis_size("ep")
    own_width = model_width // tp_count
    top_count = route_ids.shape[1]
    block_units = w_down.shape[0]
    span_count = FF // block_units
    experts = ep_count // span_count
    slot_cap = max(2, 3 * seq_count * top_count // (2 * experts))
    residual_in = tokens.astype(jnp.float32)
    normed = scaled_rows(residual_in, jnp.sum(residual_in * residual_in, 1), model_width, mix_gain)

    def project(weight):
        product = jnp.dot(normed, weight, preferred_element_type=jnp.float32)
        return rounded_wide(product).reshape(seq_count, local_heads, head_dim)

    query_rows = project(w_query)
    key_rows = project(w_key) * head_dim ** (-0.5)
    value_rows = project(w_value)
    head_start = tp_at * local_heads
    input_gate = lax.dynamic_slice_in_dim(
        jnp.dot(normed, w_igate, preferred_element_type=jnp.float32), head_start, local_heads, 1
    )
    forget_pre = jnp.dot(normed, w_fgate, preferred_element_type=jnp.float32) + forget_bias[None, :]
    forget_log = jax.nn.log_sigmoid(
        lax.dynamic_slice_in_dim(forget_pre, head_start, local_heads, 1)
    )
    new_max = jnp.maximum(forget_log + max_state, input_gate)
    keep_weight = jnp.exp(forget_log + max_state - new_max)
    new_weight = jnp.exp(input_gate - new_max)
    memory = mem_state.reshape(seq_count, local_heads, head_dim, head_dim)
    new_memory = (
        keep_weight[:, :, None, None] * memory
        + new_weight[:, :, None, None] * key_rows[:, :, :, None] * value_rows[:, :, None, :]
    )
    new_norm = (
        keep_weight[:, :, None] * norm_state.reshape(seq_count, local_heads, head_dim)
        + new_weight[:, :, None] * key_rows
    )
    numerator = jnp.einsum("shd,shde->she", query_rows, new_memory, precision=lax.Precision.HIGHEST)
    denominator = jnp.sum(query_rows * new_norm, axis=2)
    readout = (numerator / jnp.maximum(jnp.abs(denominator), jnp.exp(-new_max))[:, :, None]).astype(
        jnp.bfloat16
    )
    readout = readout.reshape(seq_count, local_heads * head_dim)
    partial_value = jnp.dot(readout, w_out, preferred_element_type=jnp.float32)
    head_total = lax.psum(partial_value.astype(jnp.bfloat16), "tp").astype(jnp.float32)
    residual = (residual_in + head_total).astype(jnp.bfloat16)
    residual_wide = lax.optimization_barrier(residual).astype(jnp.float32)
    outgoing = scaled_rows(
        residual_wide, jnp.sum(residual_wide * residual_wide, 1), model_width, ffn_gain
    )
    own_residual = lax.dynamic_slice_in_dim(residual, tp_at * own_width, own_width, 1)
    flat_ids = route_ids.reshape(-1)
    matches = (flat_ids[:, None] == jnp.arange(experts, dtype=jnp.int32)[None, :]).astype(jnp.int32)
    slot_rank = jnp.sum((jnp.cumsum(matches, 0) - matches) * matches, 1)
    slot_index = (flat_ids * slot_cap + slot_rank).reshape(seq_count, top_count)
    chosen = (
        slot_index[:, :, None] == jnp.arange(experts * slot_cap, dtype=jnp.int32)[None, None, :]
    ).astype(jnp.float32)
    placing = jnp.sum(chosen, 1).astype(jnp.bfloat16)
    mixing = jnp.sum(chosen * route_weights[:, :, None], 1)
    packed = jnp.einsum("sj,sc->jc", placing, outgoing, preferred_element_type=jnp.float32).astype(
        jnp.bfloat16
    )
    packed_width = packed.shape[1]
    outbound = jnp.broadcast_to(
        packed.reshape(experts, 1, slot_cap, packed_width),
        (experts, span_count, slot_cap, packed_width),
    ).reshape(ep_count, slot_cap, packed_width)
    arrived = lax.all_to_all(outbound, "ep", split_axis=0, concat_axis=0, tiled=True)
    sources = arrived.shape[0]
    item_count = arrived.shape[1]
    flat_rows = arrived.reshape(sources * item_count, arrived.shape[2])
    gate_sum = jnp.dot(flat_rows, w_gate, preferred_element_type=jnp.float32)
    up_sum = jnp.dot(flat_rows, w_up, preferred_element_type=jnp.float32)
    hidden = (jax.nn.silu(gate_sum) * up_sum).astype(jnp.bfloat16)
    partial_out = jnp.dot(
        lax.all_gather(hidden, "tp", axis=1, tiled=True), w_down, preferred_element_type=jnp.float32
    )
    returned = lax.all_to_all(
        partial_out.reshape(sources, item_count, w_down.shape[1]).astype(jnp.bfloat16),
        "ep",
        split_axis=0,
        concat_axis=0,
        tiled=True,
    ).astype(jnp.float32)
    results = jnp.sum(returned.reshape(experts, span_count, slot_cap, own_width), 1).reshape(
        experts * slot_cap, own_width
    )
    routed = jnp.dot(
        mixing, results, precision=lax.Precision.HIGHEST, preferred_element_type=jnp.float32
    )
    out_tokens = (own_residual.astype(jnp.float32) + routed).astype(jnp.bfloat16)
    return (
        out_tokens,
        new_memory.reshape(seq_count, local_heads, head_dim * head_dim),
        new_norm.reshape(seq_count, local_heads * head_dim),
        new_max,
    )


def solution(mesh):
    placed = (
        P("ep", None),
        P(),
        P(None, "tp"),
        P(None, "tp"),
        P(None, "tp"),
        P(),
        P(),
        P(),
        P("tp", None),
        P("ep", "tp", None),
        P("ep", "tp"),
        P("ep", "tp"),
        P(),
        P("ep", None),
        P("ep", None),
        P(None, ("ep", "tp")),
        P(None, ("ep", "tp")),
        P("ep", "tp"),
    )
    return jax.shard_map(
        shards,
        mesh=mesh,
        in_specs=placed,
        out_specs=(P("ep", "tp"), P("ep", "tp", None), P("ep", "tp"), P("ep", "tp")),
        check_vma=False,
    )
```

profile of v0, /device:TPU:0, one launch (start us, length us, event | category | flops | bytes accessed | tf_op | source)
XLA Modules:
  0.0 65.1 jit_solution(17769218186569641081)
XLA Ops:
  0.6 0.9 %fusion.9 = f32[8]{0:T(128)S(1)} fusion(bf16[8,2048]{1,0:T(8,128)(2,1)} %param.18), kind=kLoop, calls=%fused_computation.25 | loop fusion | flops 49144 | bytes 32800 | tf_op jit(solution)/shard_map/reduce_sum | solution.py:52
  1.6 0.8 %copy.36 = s32[8,2]{1,0:T(8,128)S(1)} copy(s32[8,2]{0,1:T(2,128)} %param.31) | data formatting | bytes 128 | tf_op args[13]
  2.4 0.7 %copy.34 = f32[8,1]{1,0:T(8,128)S(1)} copy(f32[8,1]{0,1:T(1,128)} %param.29) | data formatting | bytes 64 | tf_op args[11]
  3.2 0.7 %convert_element_type.78 = f32[2048]{0:T(1024)S(1)} convert(bf16[2048]{0:T(1024)(128)(2,1)} %param.19) | non-fusion elementwise | flops 2048 | bytes 12288 | tf_op jit(solution)/shard_map/convert_element_type | solution.py:12
  3.9 1.3 %convolution_convert_fusion.4 = bf16[8,128]{1,0:T(8,128)(2,1)S(1)} fusion(bf16[2048,128]{1,0:T(8,128)(2,1)} %param.21, bf16[8,2048]{1,0:T(8,128)(2,1)} %param.18, f32[2048]{0:T(1024)S(1)} %convert_element_type.78, f32[8]{0:T(128)S(1)} %add_rsqrt_fusion.1), kind=kOutput, calls=%fused_computation.9 | convolution fusion | flops 4260864 | bytes 567328 | tf_op jit(solution)/shard_map/dot_general | solution.py:55
  5.2 1.3 %convolution_convert_fusion.3 = bf16[8,128]{1,0:T(8,128)(2,1)S(1)} fusion(bf16[2048,128]{1,0:T(8,128)(2,1)} %param.22, bf16[8,2048]{1,0:T(8,128)(2,1)} %param.18, f32[2048]{0:T(1024)S(1)} %convert_element_type.78, f32[8]{0:T(128)S(1)} %add_rsqrt_fusion.1), kind=kOutput, calls=%fused_computation.8 | convolution fusion | flops 4260864 | bytes 567328 | tf_op jit(solution)/shard_map/dot_general | solution.py:55
  6.5 1.3 %convolution_convert_fusion.5 = bf16[8,128]{1,0:T(8,128)(2,1)S(1)} fusion(bf16[2048,128]{1,0:T(8,128)(2,1)} %param.20, bf16[8,2048]{1,0:T(8,128)(2,1)} %param.18, f32[2048]{0:T(1024)S(1)} %convert_element_type.78, f32[8]{0:T(128)S(1)} %add_rsqrt_fusion.1), kind=kOutput, calls=%fused_computation.10 | convolution fusion | flops 4260864 | bytes 567328 | tf_op jit(solution)/shard_map/dot_general | solution.py:55
  7.8 1.0 %fusion.24 = f32[8,4]{1,0:T(8,128)S(1)} fusion(bf16[2048,4]{0,1:T(4,128)(2,1)} %param.23, bf16[8,2048]{1,0:T(8,128)(2,1)} %param.18, f32[2048]{0:T(1024)S(1)} %convert_element_type.78, f32[8]{0:T(128)S(1)} %add_rsqrt_fusion.1), kind=kOutput, calls=%fused_computation.55 | convolution fusion | flops 196608 | bytes 57504 | tf_op jit(solution)/shard_map/dot_general | solution.py:63
  8.7 1.0 %convolution_add_fusion.1 = f32[8,4]{1,0:T(8,128)S(1)} fusion(bf16[2048,4]{0,1:T(4,128)(2,1)} %param.24, f32[4]{0:T(128)} %param.25, bf16[8,2048]{1,0:T(8,128)(2,1)} %param.18, f32[2048]{0:T(1024)S(1)} %convert_element_type.78, f32[8]{0:T(128)S(1)} %add_rsqrt_fusion.1), kind=kOutput, calls=%fused_computation.7 | convolution fusion | flops 196640 | bytes 57520 | tf_op jit(solution)/shard_map/dot_general | solution.py:65
  9.9 1.5 %multiply_reduce_fusion = (f32[8]{0:T(128)S(1)}, f32[8,128]{1,0:T(8,128)}, f32[8,128]{1,0:T(8,128)S(1)}) fusion(bf16[8,128]{1,0:T(8,128)(2,1)S(1)} %convolution_convert_fusion.5, f32[8]{0:T(128)S(1)} %get-tuple-element.16, bf16[8,128]{1,0:T(8,128)(2,1)S(1)} %convolution_convert_fusion.4, f32[8,128]{1,0:T(8,128)} %param.28, f32[8]{0:T(128)S(1)} %get-tuple-element.17), kind=kLoop, calls=%fused_computation.44 | loop fusion | flops 7160 | bytes 16480 | tf_op jit(solution)/shard_map/reduce_sum | solution.py:82
  12.0 0.7 %convert_element_type.95 = f32[2048]{0:T(1024)S(1)} convert(bf16[2048]{0:T(1024)(128)(2,1)} %param.30) | non-fusion elementwise | flops 2048 | bytes 12288 | tf_op jit(solution)/shard_map/convert_element_type | solution.py:12
  12.8 1.5 %fusion.2 = f32[8,1,128]{2,1,0:T(1,128)S(1)} fusion(f32[8,128,128]{2,1,0:T(8,128)} %bitcast.22, f32[8]{0:T(128)S(1)} %get-tuple-element.17, f32[8,128]{1,0:T(8,128)S(1)} %convert_element_type.84, f32[8,128]{1,0:T(8,128)S(1)} %get-tuple-element.23, bf16[8,128,1]{1,0,2:T(8,128)(2,1)S(1)} %bitcast.24), kind=kOutput, calls=%fused_computation.12 | convolution fusion | flops 1966080 | bytes 538656 | tf_op jit(solution)/shard_map/shd,shde->she/dot_general | solution.py:81
  14.5 12.9 %psum.7 = bf16[8,2048]{1,0:T(8,128)(2,1)S(1)} all-reduce(bf16[8,2048]{1,0:T(8,128)(2,1)S(1)} %convolution_convert_fusion.1), channel_id=1, replica_groups=mesh['ep'=8,'tp'=4] {'tp'}, use_global_device_ids=true, to_apply=%region_2.3 | all-reduce | flops 16384 | bytes 65536 | tf_op jit(solution)/shard_map/psum | solution.py:88
  27.5 0.8 %fusion.12 = bf16[8,2048]{1,0:T(8,128)(2,1)S(1)} fusion(bf16[8,2048]{1,0:T(8,128)(2,1)} %param.18, bf16[8,2048]{1,0:T(8,128)(2,1)S(1)} %psum.7), kind=kLoop, calls=%fused_computation.28 | loop fusion | flops 65536 | bytes 98304 | tf_op jit(solution)/shard_map/convert_element_type | solution.py:89
  28.4 0.8 %convert_reduce_fusion = (bf16[8,24]{1,0:T(8,128)(2,1)S(1)}, f32[8,24]{1,0:T(8,128)S(1)}) fusion(s32[8,2]{0,1:T(2,128)S(1)} %copy.38, f32[8,2]{0,1:T(2,128)} %param.32), kind=kLoop, calls=%fused_computation.32 | loop fusion | flops 1536 | bytes 1280 | tf_op jit(solution)/shard_map/reduce_sum | solution.py:102
  29.4 0.7 %reshape_reshape.3 = bf16[8,3,2048]{2,1,0:T(4,128)(2,1)} reshape(bf16[24,2048]{1,0:T(8,128)(2,1)S(1)} %convolution_convert_fusion) | data formatting | bytes 196608 | tf_op jit(solution)/shard_map/reshape;reshape | solution.py:111
  30.1 5.8 %all-to-all-start = ((bf16[8,3,2048]{2,1,0:T(4,128)(2,1)}), bf16[8,3,2048]{2,1,0:T(4,128)(2,1)S(1)}, u32[]{:S(2)}, u32[]{:S(2)}) async-start(bf16[8,3,2048]{2,1,0:T(4,128)(2,1)} %reshape_reshape.3), calls=%async_computation | async-start | bytes 262144 | tf_op jit(solution)/shard_map/all_to_all | solution.py:112
  36.1 7.1 %all-to-all-done = bf16[8,3,2048]{2,1,0:T(4,128)(2,1)S(1)} async-done(((bf16[8,3,2048]{2,1,0:T(4,128)(2,1)}), bf16[8,3,2048]{2,1,0:T(4,128)(2,1)S(1)}, u32[]{:S(2)}, u32[]{:S(2)}) %all-to-all-start) | async-done | bytes 98336 | tf_op jit(solution)/shard_map/all_to_all | solution.py:112
  43.4 3.0 %fusion.28 = f32[24,1024]{1,0:T(8,128)S(1)} fusion(bf16[24,2048]{1,0:T(8,128)(2,1)S(1)} %reshape.138, bf16[2048,1024]{1,0:T(8,128)(2,1)} %param.33), kind=kOutput, calls=%fused_computation.56 | convolution fusion | flops 100663296 | bytes 4390912 | tf_op jit(solution)/shard_map/dot_general | solution.py:116
  47.5 5.6 %all_gather.3 = bf16[24,4096]{1,0:T(8,128)(2,1)S(1)} all-gather(bf16[24,1024]{1,0:T(8,128)(2,1)S(1)} %fusion), channel_id=1, replica_groups=mesh['ep'=8,'tp'=4] {'tp'}, dimensions={1}, use_global_device_ids=true | all-gather | bytes 245760 | tf_op jit(solution)/shard_map/all_gather | solution.py:120
  54.4 3.3 %all-to-all-start.1 = ((bf16[8,3,512]{2,1,0:T(4,128)(2,1)}), bf16[8,3,512]{2,1,0:T(4,128)(2,1)S(1)}, u32[]{:S(2)}, u32[]{:S(2)}) async-start(bf16[8,3,512]{2,1,0:T(4,128)(2,1)} %convert_element_type.100), calls=%async_computation.1 | async-start | bytes 65536 | tf_op jit(solution)/shard_map/all_to_all | solution.py:122
  57.7 1.4 %multiply_add_fusion = f32[8,1,16384]{2,1,0:T(1,128)} fusion(f32[8,1,16384]{2,1,0:T(1,128)S(1)} %bitcast.23, f32[8,1,16384]{2,1,0:T(1,128)S(1)} %copy-done.3, f32[8]{0:T(128)S(1)} %get-tuple-element.17), kind=kLoop, calls=%fused_computation.11 | loop fusion | flops 262144 | bytes 1572896 | tf_op jit(solution)/shard_map/add | solution.py:74
  59.7 4.6 %all-to-all-done.1 = bf16[8,3,512]{2,1,0:T(4,128)(2,1)S(1)} async-done(((bf16[8,3,512]{2,1,0:T(4,128)(2,1)}), bf16[8,3,512]{2,1,0:T(4,128)(2,1)S(1)}, u32[]{:S(2)}, u32[]{:S(2)}) %all-to-all-start.1) | async-done | bytes 24608 | tf_op jit(solution)/shard_map/all_to_all | solution.py:122
  64.4 0.7 %fusion.1 = bf16[8,512]{1,0:T(8,128)(2,1)} fusion(f32[8,24]{1,0:T(8,128)S(1)} %get-tuple-element.19, bf16[24,512]{1,0:T(8,128)(2,1)S(1)} %reshape.139, bf16[8,2048]{1,0:T(8,128)(2,1)S(1)} %fusion.12, s32[]{:T(128)S(6)} %select_n.14), kind=kOutput, calls=%fused_computation.6 | convolution fusion | flops 1191936 | bytes 41732 | tf_op jit(solution)/shard_map/dot_general | solution.py:132
  (32 shorter events, 4.9 us)
Async XLA Ops:
  0.6 13.7 %copy-start = (bf16[128,2048]{1,0:T(8,128)(2,1)S(1)}, bf16[128,2048]{1,0:T(8,128)(2,1)}, u32[]{:S(2)}) copy-start(bf16[128,2048]{1,0:T(8,128)(2,1)} %param.26) | copy-start | bytes 1572868
  30.1 13.1 %all-to-all-start = ((bf16[8,3,2048]{2,1,0:T(4,128)(2,1)}), bf16[8,3,2048]{2,1,0:T(4,128)(2,1)S(1)}, u32[]{:S(2)}, u32[]{:S(2)}) async-start(bf16[8,3,2048]{2,1,0:T(4,128)(2,1)} %reshape_reshape.3), calls=%async_computation | async-start | bytes 262144 | tf_op jit(solution)/shard_map/all_to_all | solution.py:112
  43.4 3.5 %copy-start.1 = (bf16[2048,1024]{1,0:T(8,128)(2,1)S(1)}, bf16[2048,1024]{1,0:T(8,128)(2,1)}, u32[]{:S(2)}) copy-start(bf16[2048,1024]{1,0:T(8,128)(2,1)} %param.34) | copy-start | bytes 12582916
  43.4 9.7 %copy-start.2 = (bf16[4096,512]{1,0:T(8,128)(2,1)S(1)}, bf16[4096,512]{1,0:T(8,128)(2,1)}, u32[]{:S(2)}) copy-start(bf16[4096,512]{1,0:T(8,128)(2,1)} %param.35) | copy-start | bytes 12582916
  46.8 10.9 %copy-start.3 = (f32[8,1,16384]{2,1,0:T(1,128)S(1)}, f32[8,1,16384]{2,1,0:T(1,128)}, u32[]{:S(2)}) copy-start(f32[8,1,16384]{2,1,0:T(1,128)} %param.27) | copy-start | bytes 1572868
  54.4 10.0 %all-to-all-start.1 = ((bf16[8,3,512]{2,1,0:T(4,128)(2,1)}), bf16[8,3,512]{2,1,0:T(4,128)(2,1)S(1)}, u32[]{:S(2)}, u32[]{:S(2)}) async-start(bf16[8,3,512]{2,1,0:T(4,128)(2,1)} %convert_element_type.100), calls=%async_computation.1 | async-start | bytes 65536 | tf_op jit(solution)/shard_map/all_to_all | solution.py:122
where the time goes:
time: 65.9 us; the launch traced here: 65.1 us
  blocking collectives  18.5 us (28%)
  matrix products  12.9 us (20%)
  waiting for transfers between devices  11.8 us (18%)
  starting transfers between devices  9.14 us (14%)
  other arithmetic  7.75 us (12%)
  local copies, waits for them, and re-layouts  4.36 us (7%)
  between operations  0.72 us (1%)
    psum x1, blocking collectives, shards(): lax.psum(partial_value.astype(jnp.bfloat16), 'tp').astype(jnp.float32)  12.9 us
    all_to_all x1, waiting for transfers between devices, shards(): lax.all_to_all(outbound, 'ep', split_axis=0, concat_axis=0, tiled=True)  7.14 us
    all_to_all x1, starting transfers between devices, shards(): lax.all_to_all(outbound, 'ep', split_axis=0, concat_axis=0, tiled=True)  5.8 us
    all_gather x1, blocking collectives, shards(): lax.all_gather(hidden, 'tp', axis=1, tiled=True)  5.59 us
    all_to_all x1, waiting for transfers between devices, shards(): lax.all_to_all(partial_out.reshape(sources, item_count, w_down.shape[1])....  4.63 us
    dot_general x3, matrix products, project(): product = jnp.dot(normed, weight, preferred_element_type=jnp.float32)  3.89 us
    all_to_all x1, starting transfers between devices, shards(): lax.all_to_all(partial_out.reshape(sources, item_count, w_down.shape[1])....  3.33 us
    dot_general x1, matrix products, shards(): gate_sum = jnp.dot(flat_rows, w_gate, preferred_element_type=jnp.float32)  2.99 us
  transfers between devices with their start and end apart: 2, of which 2 were waited for; matrix products, arithmetic and copies ran while one was open for 3% of the time, Pallas kernels for 0%

commit v1 on v0

--- a/solution.py
+++ b/solution.py
@@ -85,7 +85,9 @@
     )
     readout = readout.reshape(seq_count, local_heads * head_dim)
     partial_value = jnp.dot(readout, w_out, preferred_element_type=jnp.float32)
-    head_total = lax.psum(partial_value.astype(jnp.bfloat16), "tp").astype(jnp.float32)
+    head_total = jnp.sum(lax.all_gather(partial_value.astype(jnp.bfloat16), "tp"), axis=0).astype(
+        jnp.float32
+    )
     residual = (residual_in + head_total).astype(jnp.bfloat16)
     residual_wide = lax.optimization_barrier(residual).astype(jnp.float32)
     outgoing = scaled_rows(

time: 65.9 us -> 60 us (0.910)
  blocking collectives: 18.5 us -> 12.1 us
    psum x1 -> x0, blocking collectives: 12.9 us -> none  [shards(): lax.psum(partial_value.astype(jnp.bfloat16), 'tp').astype(jnp.float32)]
    all_gather x0 -> x1, blocking collectives: none -> 6.54 us  [shards(): lax.all_gather(partial_value.astype(jnp.bfloat16), 'tp')]
  transfers between devices with their start and end apart: 2 -> 2, of which waited for: 2 -> 2; matrix products, arithmetic and copies ran while one was open for 3% -> 4% of each run, Pallas kernels for 0% -> 0%
where the time goes in v1:
time: 60 us; the launch traced here: 59.2 us
  matrix products  12.9 us (22%)
  blocking collectives  12.1 us (20%)
  waiting for transfers between devices  11.9 us (20%)
  starting transfers between devices  9.49 us (16%)
  other arithmetic  7.77 us (13%)
  local copies, waits for them, and re-layouts  4.36 us (7%)
  between operations  0.71 us (1%)
    all_to_all x1, waiting for transfers between devices, shards(): lax.all_to_all(outbound, 'ep', split_axis=0, concat_axis=0, tiled=True)  7.29 us
    all_gather x1, blocking collectives, shards(): lax.all_gather(partial_value.astype(jnp.bfloat16), 'tp')  6.54 us
    all_to_all x1, starting transfers between devices, shards(): lax.all_to_all(outbound, 'ep', split_axis=0, concat_axis=0, tiled=True)  6.16 us
    all_gather x1, blocking collectives, shards(): lax.all_gather(hidden, 'tp', axis=1, tiled=True)  5.59 us
    all_to_all x1, waiting for transfers between devices, shards(): lax.all_to_all(partial_out.reshape(sources, item_count, w_down.shape[1])....  4.63 us
    dot_general x3, matrix products, project(): product = jnp.dot(normed, weight, preferred_element_type=jnp.float32)  3.89 us
    all_to_all x1, starting transfers between devices, shards(): lax.all_to_all(partial_out.reshape(sources, item_count, w_down.shape[1])....  3.33 us
    dot_general x1, matrix products, shards(): gate_sum = jnp.dot(flat_rows, w_gate, preferred_element_type=jnp.float32)  2.99 us
  transfers between devices with their start and end apart: 2, of which 2 were waited for; matrix products, arithmetic and copies ran while one was open for 4% of the time, Pallas kernels for 0%

profile of v1, /device:TPU:0, one launch (start us, length us, event | category | flops | bytes accessed | tf_op | source)
XLA Modules:
  0.0 59.2 jit_solution(16486959475970519774)
XLA Ops:
  0.6 0.9 %fusion.9 = f32[8]{0:T(128)S(1)} fusion(bf16[8,2048]{1,0:T(8,128)(2,1)} %param.18), kind=kLoop, calls=%fused_computation.26 | loop fusion | flops 49144 | bytes 32800 | tf_op jit(solution)/shard_map/reduce_sum | solution.py:52
  1.6 0.8 %copy.36 = s32[8,2]{1,0:T(8,128)S(1)} copy(s32[8,2]{0,1:T(2,128)} %param.31) | data formatting | bytes 128 | tf_op args[13]
  2.4 0.7 %copy.34 = f32[8,1]{1,0:T(8,128)S(1)} copy(f32[8,1]{0,1:T(1,128)} %param.29) | data formatting | bytes 64 | tf_op args[11]
  3.2 0.7 %convert_element_type.80 = f32[2048]{0:T(1024)S(1)} convert(bf16[2048]{0:T(1024)(128)(2,1)} %param.19) | non-fusion elementwise | flops 2048 | bytes 12288 | tf_op jit(solution)/shard_map/convert_element_type | solution.py:12
  3.9 1.3 %convolution_convert_fusion.4 = bf16[8,128]{1,0:T(8,128)(2,1)S(1)} fusion(bf16[2048,128]{1,0:T(8,128)(2,1)} %param.21, bf16[8,2048]{1,0:T(8,128)(2,1)} %param.18, f32[2048]{0:T(1024)S(1)} %convert_element_type.80, f32[8]{0:T(128)S(1)} %add_rsqrt_fusion.1), kind=kOutput, calls=%fused_computation.9 | convolution fusion | flops 4260864 | bytes 567328 | tf_op jit(solution)/shard_map/dot_general | solution.py:55
  5.2 1.3 %convolution_convert_fusion.3 = bf16[8,128]{1,0:T(8,128)(2,1)S(1)} fusion(bf16[2048,128]{1,0:T(8,128)(2,1)} %param.22, bf16[8,2048]{1,0:T(8,128)(2,1)} %param.18, f32[2048]{0:T(1024)S(1)} %convert_element_type.80, f32[8]{0:T(128)S(1)} %add_rsqrt_fusion.1), kind=kOutput, calls=%fused_computation.8 | convolution fusion | flops 4260864 | bytes 567328 | tf_op jit(solution)/shard_map/dot_general | solution.py:55
  6.5 1.3 %convolution_convert_fusion.5 = bf16[8,128]{1,0:T(8,128)(2,1)S(1)} fusion(bf16[2048,128]{1,0:T(8,128)(2,1)} %param.20, bf16[8,2048]{1,0:T(8,128)(2,1)} %param.18, f32[2048]{0:T(1024)S(1)} %convert_element_type.80, f32[8]{0:T(128)S(1)} %add_rsqrt_fusion.1), kind=kOutput, calls=%fused_computation.10 | convolution fusion | flops 4260864 | bytes 567328 | tf_op jit(solution)/shard_map/dot_general | solution.py:55
  7.8 1.0 %fusion.24 = f32[8,4]{1,0:T(8,128)S(1)} fusion(bf16[2048,4]{0,1:T(4,128)(2,1)} %param.23, bf16[8,2048]{1,0:T(8,128)(2,1)} %param.18, f32[2048]{0:T(1024)S(1)} %convert_element_type.80, f32[8]{0:T(128)S(1)} %add_rsqrt_fusion.1), kind=kOutput, calls=%fused_computation.56 | convolution fusion | flops 196608 | bytes 57504 | tf_op jit(solution)/shard_map/dot_general | solution.py:63
  8.7 1.0 %convolution_add_fusion.1 = f32[8,4]{1,0:T(8,128)S(1)} fusion(bf16[2048,4]{0,1:T(4,128)(2,1)} %param.24, f32[4]{0:T(128)} %param.25, bf16[8,2048]{1,0:T(8,128)(2,1)} %param.18, f32[2048]{0:T(1024)S(1)} %convert_element_type.80, f32[8]{0:T(128)S(1)} %add_rsqrt_fusion.1), kind=kOutput, calls=%fused_computation.7 | convolution fusion | flops 196640 | bytes 57520 | tf_op jit(solution)/shard_map/dot_general | solution.py:65
  9.9 1.5 %multiply_reduce_fusion = (f32[8]{0:T(128)S(1)}, f32[8,128]{1,0:T(8,128)}, f32[8,128]{1,0:T(8,128)S(1)}) fusion(bf16[8,128]{1,0:T(8,128)(2,1)S(1)} %convolution_convert_fusion.5, f32[8]{0:T(128)S(1)} %get-tuple-element.16, bf16[8,128]{1,0:T(8,128)(2,1)S(1)} %convolution_convert_fusion.4, f32[8,128]{1,0:T(8,128)} %param.28, f32[8]{0:T(128)S(1)} %get-tuple-element.17), kind=kLoop, calls=%fused_computation.45 | loop fusion | flops 7160 | bytes 16480 | tf_op jit(solution)/shard_map/reduce_sum | solution.py:82
  12.0 0.7 %convert_element_type.97 = f32[2048]{0:T(1024)S(1)} convert(bf16[2048]{0:T(1024)(128)(2,1)} %param.30) | non-fusion elementwise | flops 2048 | bytes 12288 | tf_op jit(solution)/shard_map/convert_element_type | solution.py:12
  12.8 1.5 %fusion.2 = f32[8,1,128]{2,1,0:T(1,128)S(1)} fusion(f32[8,128,128]{2,1,0:T(8,128)} %bitcast.24, f32[8]{0:T(128)S(1)} %get-tuple-element.17, f32[8,128]{1,0:T(8,128)S(1)} %convert_element_type.86, f32[8,128]{1,0:T(8,128)S(1)} %get-tuple-element.23, bf16[8,128,1]{1,0,2:T(8,128)(2,1)S(1)} %bitcast.26), kind=kOutput, calls=%fused_computation.12 | convolution fusion | flops 1966080 | bytes 538656 | tf_op jit(solution)/shard_map/shd,shde->she/dot_general | solution.py:81
  14.5 6.5 %all-gather = bf16[32,2048]{1,0:T(8,128)(2,1)S(1)} all-gather(bf16[8,2048]{1,0:T(8,128)(2,1)S(1)} %convolution_convert_fusion.1), channel_id=2, replica_groups=mesh['ep'=8,'tp'=4] {'tp'}, dimensions={0}, use_global_device_ids=true | all-gather | bytes 163840 | tf_op jit(solution)/shard_map/all_gather | solution.py:88
  21.1 0.8 %fusion.12 = bf16[8,2048]{1,0:T(8,128)(2,1)S(1)} fusion(bf16[8,2048]{1,0:T(8,128)(2,1)} %param.18, bf16[8,2048]{1,0:T(8,128)(2,1)S(1)} %bitcast_reduce_fusion), kind=kLoop, calls=%fused_computation.29 | loop fusion | flops 65536 | bytes 98304 | tf_op jit(solution)/shard_map/convert_element_type | solution.py:91
  22.0 0.8 %convert_reduce_fusion = (bf16[8,24]{1,0:T(8,128)(2,1)S(1)}, f32[8,24]{1,0:T(8,128)S(1)}) fusion(s32[8,2]{0,1:T(2,128)S(1)} %copy.38, f32[8,2]{0,1:T(2,128)} %param.32), kind=kLoop, calls=%fused_computation.33 | loop fusion | flops 1536 | bytes 1280 | tf_op jit(solution)/shard_map/reduce_sum | solution.py:104
  23.0 0.7 %reshape_reshape.3 = bf16[8,3,2048]{2,1,0:T(4,128)(2,1)} reshape(bf16[24,2048]{1,0:T(8,128)(2,1)S(1)} %convolution_convert_fusion) | data formatting | bytes 196608 | tf_op jit(solution)/shard_map/reshape;reshape | solution.py:113
  23.7 6.2 %all-to-all-start = ((bf16[8,3,2048]{2,1,0:T(4,128)(2,1)}), bf16[8,3,2048]{2,1,0:T(4,128)(2,1)S(1)}, u32[]{:S(2)}, u32[]{:S(2)}) async-start(bf16[8,3,2048]{2,1,0:T(4,128)(2,1)} %reshape_reshape.3), calls=%async_computation | async-start | bytes 262144 | tf_op jit(solution)/shard_map/all_to_all | solution.py:114
  30.1 7.3 %all-to-all-done = bf16[8,3,2048]{2,1,0:T(4,128)(2,1)S(1)} async-done(((bf16[8,3,2048]{2,1,0:T(4,128)(2,1)}), bf16[8,3,2048]{2,1,0:T(4,128)(2,1)S(1)}, u32[]{:S(2)}, u32[]{:S(2)}) %all-to-all-start) | async-done | bytes 98336 | tf_op jit(solution)/shard_map/all_to_all | solution.py:114
  37.5 3.0 %fusion.28 = f32[24,1024]{1,0:T(8,128)S(1)} fusion(bf16[24,2048]{1,0:T(8,128)(2,1)S(1)} %reshape.138, bf16[2048,1024]{1,0:T(8,128)(2,1)} %param.33), kind=kOutput, calls=%fused_computation.57 | convolution fusion | flops 100663296 | bytes 4390912 | tf_op jit(solution)/shard_map/dot_general | solution.py:118
  41.6 5.6 %all_gather.11 = bf16[24,4096]{1,0:T(8,128)(2,1)S(1)} all-gather(bf16[24,1024]{1,0:T(8,128)(2,1)S(1)} %fusion), channel_id=1, replica_groups=mesh['ep'=8,'tp'=4] {'tp'}, dimensions={1}, use_global_device_ids=true | all-gather | bytes 245760 | tf_op jit(solution)/shard_map/all_gather | solution.py:122
  48.5 3.3 %all-to-all-start.1 = ((bf16[8,3,512]{2,1,0:T(4,128)(2,1)}), bf16[8,3,512]{2,1,0:T(4,128)(2,1)S(1)}, u32[]{:S(2)}, u32[]{:S(2)}) async-start(bf16[8,3,512]{2,1,0:T(4,128)(2,1)} %convert_element_type.102), calls=%async_computation.1 | async-start | bytes 65536 | tf_op jit(solution)/shard_map/all_to_all | solution.py:124
  51.8 1.4 %multiply_add_fusion = f32[8,1,16384]{2,1,0:T(1,128)} fusion(f32[8,1,16384]{2,1,0:T(1,128)S(1)} %bitcast.25, f32[8,1,16384]{2,1,0:T(1,128)S(1)} %copy-done.3, f32[8]{0:T(128)S(1)} %get-tuple-element.17), kind=kLoop, calls=%fused_computation.11 | loop fusion | flops 262144 | bytes 1572896 | tf_op jit(solution)/shard_map/add | solution.py:74
  53.8 4.6 %all-to-all-done.1 = bf16[8,3,512]{2,1,0:T(4,128)(2,1)S(1)} async-done(((bf16[8,3,512]{2,1,0:T(4,128)(2,1)}), bf16[8,3,512]{2,1,0:T(4,128)(2,1)S(1)}, u32[]{:S(2)}, u32[]{:S(2)}) %all-to-all-start.1) | async-done | bytes 24608 | tf_op jit(solution)/shard_map/all_to_all | solution.py:124
  58.5 0.7 %fusion.1 = bf16[8,512]{1,0:T(8,128)(2,1)} fusion(f32[8,24]{1,0:T(8,128)S(1)} %get-tuple-element.19, bf16[24,512]{1,0:T(8,128)(2,1)S(1)} %reshape.139, bf16[8,2048]{1,0:T(8,128)(2,1)S(1)} %fusion.12, s32[]{:T(128)S(6)} %select_n.14), kind=kOutput, calls=%fused_computation.6 | convolution fusion | flops 1191936 | bytes 41732 | tf_op jit(solution)/shard_map/dot_general | solution.py:134
  (33 shorter events, 4.9 us)
Async XLA Ops:
  0.6 13.7 %copy-start = (bf16[128,2048]{1,0:T(8,128)(2,1)S(1)}, bf16[128,2048]{1,0:T(8,128)(2,1)}, u32[]{:S(2)}) copy-start(bf16[128,2048]{1,0:T(8,128)(2,1)} %param.26) | copy-start | bytes 1572868
  23.7 13.7 %all-to-all-start = ((bf16[8,3,2048]{2,1,0:T(4,128)(2,1)}), bf16[8,3,2048]{2,1,0:T(4,128)(2,1)S(1)}, u32[]{:S(2)}, u32[]{:S(2)}) async-start(bf16[8,3,2048]{2,1,0:T(4,128)(2,1)} %reshape_reshape.3), calls=%async_computation | async-start | bytes 262144 | tf_op jit(solution)/shard_map/all_to_all | solution.py:114
  37.5 3.5 %copy-start.1 = (bf16[2048,1024]{1,0:T(8,128)(2,1)S(1)}, bf16[2048,1024]{1,0:T(8,128)(2,1)}, u32[]{:S(2)}) copy-start(bf16[2048,1024]{1,0:T(8,128)(2,1)} %param.34) | copy-start | bytes 12582916
  37.5 9.7 %copy-start.2 = (bf16[4096,512]{1,0:T(8,128)(2,1)S(1)}, bf16[4096,512]{1,0:T(8,128)(2,1)}, u32[]{:S(2)}) copy-start(bf16[4096,512]{1,0:T(8,128)(2,1)} %param.35) | copy-start | bytes 12582916
  40.9 10.9 %copy-start.3 = (f32[8,1,16384]{2,1,0:T(1,128)S(1)}, f32[8,1,16384]{2,1,0:T(1,128)}, u32[]{:S(2)}) copy-start(f32[8,1,16384]{2,1,0:T(1,128)} %param.27) | copy-start | bytes 1572868
  48.5 10.0 %all-to-all-start.1 = ((bf16[8,3,512]{2,1,0:T(4,128)(2,1)}), bf16[8,3,512]{2,1,0:T(4,128)(2,1)S(1)}, u32[]{:S(2)}, u32[]{:S(2)}) async-start(bf16[8,3,512]{2,1,0:T(4,128)(2,1)} %convert_element_type.102), calls=%async_computation.1 | async-start | bytes 65536 | tf_op jit(solution)/shard_map/all_to_all | solution.py:124
